TPU v7x, 32 devices: a whole 2x2x4 slice. The times are simulated.
32 devices in a mesh: sp: 4 (over z), tp: 4 (over y, x), dp: 2 (over core).
Axes of the slice: x: 2, y: 2, z: 4, core: 2. Of those that a mesh axis runs over, the one named last changes fastest.
Arguments:
- latent: bfloat16 [2, 3072, 2048], P('dp', ('sp', 'tp')), may hold values from -3 to 3
- cond: bfloat16 [2, 2048], P('dp', 'sp'), may hold values from -6 to 6
- cond_ctx: bfloat16 [2048], P('sp'), may hold values from -6 to 6
- context: bfloat16 [2, 512, 2048], P('dp', 'sp'), may hold values from -6 to 6
- norm_gain: bfloat16 [2048], replicated, may hold values from 0.099609375 to 1.8984375
- mod_shift: bfloat16 [2048, 2048], P('sp', 'tp'), may hold values from -0.125 to 0.125
- mod_scale: bfloat16 [2048, 2048], P('sp', 'tp'), may hold values from -0.125 to 0.125
- mod_gate: bfloat16 [2048, 2048], P('sp', 'tp'), may hold values from -0.125 to 0.125
- w_query: bfloat16 [2048, 1024], P(None, 'tp'), may hold values from -0.125 to 0.125
- w_key: bfloat16 [2048, 256], P(None, 'tp'), may hold values from -0.125 to 0.125
- w_value: bfloat16 [2048, 256], P(None, 'tp'), may hold values from -0.125 to 0.125
- q_gain: bfloat16 [64], replicated, may hold values from 1 to 5.5
- k_gain: bfloat16 [64], replicated, may hold values from 1 to 5.5
- ctx_lift: float32 [16], P('tp'), may hold values from 1 to 3
- w_out: bfloat16 [1024, 2048], replicated, may hold values from -1.5 to 1.5
Outputs:
- mixed: bfloat16 [2, 3072, 2048], P('dp', ('sp', 'tp'))
All inputs are finite; a program needn't handle non-finite values.
Results may differ from a plain program's by a relative error of at most 0.009.
The roundings to bfloat16 on the way count: a program that leaves them out, or rounds other values in their place, can miss the bound.
Values may be sent and summed in bfloat16 or wider, within the bound.
A program may use at most 64 MiB of HBM per device.

v0:
```python
import jax
import jax.numpy as jnp
from jax import lax
from jax.sharding import PartitionSpec as P

HD = 64
GRID_W = 128
EPS = 1e-06
THETA = 10000.0


def modulate(row_block, gain_vec, shift_rows, scale_rows):
    values = row_block.astype(jnp.float32)
    normed = (
        values
        * lax.rsqrt(jnp.mean(values * values, axis=-1, keepdims=True) + EPS)
        * gain_vec.astype(jnp.float32)
    )
    return (normed * (1.0 + scale_rows) + shift_rows).astype(jnp.bfloat16)


def head_norm(raw_proj, gain_vec):
    samples, tokens, width = raw_proj.shape
    pieces = raw_proj.reshape(samples, tokens, width // HD, HD)
    normed = (
        pieces
        * lax.rsqrt(jnp.mean(pieces * pieces, axis=-1, keepdims=True) + EPS)
        * gain_vec.astype(jnp.float32)
    )
    return normed.transpose(0, 2, 1, 3)


def rotate(vector, positions):
    pairs_count = vector.shape[-1] // 4
    grid_row = (positions // GRID_W).astype(jnp.float32)
    grid_col = (positions % GRID_W).astype(jnp.float32)
    inverse = THETA ** (-jnp.arange(pairs_count, dtype=jnp.float32) / pairs_count)
    angles = jnp.concatenate([grid_row[:, None] * inverse, grid_col[:, None] * inverse], axis=-1)
    cosine = jnp.cos(angles)
    sine_val = jnp.sin(angles)
    first_half = vector[..., 0::2]
    second_half = vector[..., 1::2]
    turned = jnp.stack(
        [
            first_half * cosine - second_half * sine_val,
            first_half * sine_val + second_half * cosine,
        ],
        axis=-1,
    )
    return turned.reshape(vector.shape)


def split_heads(rows):
    samples, tokens, width = rows.shape
    return rows.reshape(samples, tokens, width // HD, HD).transpose(0, 2, 1, 3)


def on_device(
    latent,
    cond,
    cond_ctx,
    context,
    norm_gain,
    mod_shift,
    mod_scale,
    mod_gate,
    w_query,
    w_key,
    w_value,
    q_gain,
    k_gain,
    ctx_lift,
    w_out,
):
    samples = latent.shape[0]
    active = jax.nn.silu(
        jnp.concatenate([cond, cond_ctx[None, :]], axis=0).astype(jnp.float32)
    ).astype(jnp.bfloat16)
    partial_mods = tuple(
        (
            jnp.dot(active, weight, preferred_element_type=jnp.float32)
            for weight in (mod_shift, mod_scale, mod_gate)
        )
    )
    summed = lax.psum(partial_mods, "sp")
    shift_rows, scale_rows, gate_rows = lax.all_gather(summed, "tp", axis=1, tiled=True)
    modulated = modulate(
        latent, norm_gain, shift_rows[:samples, None, :], scale_rows[:samples, None, :]
    )
    ctx_mod = modulate(context, norm_gain, shift_rows[samples], scale_rows[samples])
    q_width = w_query.shape[1]
    k_width = w_key.shape[1]
    w_joint = jnp.concatenate([w_query, w_key, w_value], axis=1)
    projected = jnp.einsum(
        "srd,dc->src",
        lax.all_gather(modulated, "tp", axis=1, tiled=True),
        w_joint,
        preferred_element_type=jnp.float32,
    )
    tokens = projected.shape[1]
    k_heads = k_width // HD
    group_size = q_width // k_width
    positions = lax.axis_index("sp") * tokens + jnp.arange(tokens, dtype=jnp.int32)
    queries = rotate(head_norm(projected[..., :q_width], q_gain), positions).astype(jnp.bfloat16)
    queries = queries.reshape(samples, k_heads, group_size, tokens, HD)
    key_rows = rotate(
        head_norm(projected[..., q_width : q_width + k_width], k_gain), positions
    ).astype(jnp.bfloat16)
    value_rows = split_heads(projected[..., q_width + k_width :].astype(jnp.bfloat16))
    ctx_proj = jnp.einsum(
        "srd,dc->src", ctx_mod, w_joint[:, q_width:], preferred_element_type=jnp.float32
    )
    ctx_keys = head_norm(ctx_proj[..., :k_width], k_gain).astype(jnp.bfloat16)
    ctx_values = split_heads(ctx_proj[..., k_width:].astype(jnp.bfloat16))
    lift_table = ctx_lift.reshape(1, k_heads, group_size, 1, 1)
    factor = HD ** (-0.5)

    def absorb(state_now, key_block, value_block, score_lift):
        best_old, weight_sum, accumulated = state_now
        scores = (
            jnp.einsum("skgtd,skrd->skgtr", queries, key_block, preferred_element_type=jnp.float32)
            * factor
            + score_lift
        )
        peak = jnp.maximum(best_old, jnp.max(scores, axis=-1))
        weights = jnp.exp(scores - peak[..., None])
        rescale = jnp.exp(best_old - peak)
        weight_sum = weight_sum * rescale + jnp.sum(weights, axis=-1)
        accumulated = accumulated * rescale[..., None] + jnp.einsum(
            "skgtr,skrd->skgtd",
            weights.astype(jnp.bfloat16),
            value_block,
            preferred_element_type=jnp.float32,
        )
        return (peak, weight_sum, accumulated)

    stat_shape = (samples, k_heads, group_size, tokens)
    state_now = (
        jnp.full(stat_shape, -1e30, jnp.float32),
        jnp.zeros(stat_shape, jnp.float32),
        jnp.zeros(stat_shape + (HD,), jnp.float32),
    )
    all_ctx_keys, all_ctx_values = (
        lax.all_gather(ctx_keys, "sp", axis=2, tiled=True),
        lax.all_gather(ctx_values, "sp", axis=2, tiled=True),
    )
    state_now = absorb(state_now, all_ctx_keys, all_ctx_values, lift_table)
    key_piece = lax.all_gather(key_rows, "sp", axis=2, tiled=True)
    value_piece = lax.all_gather(value_rows, "sp", axis=2, tiled=True)
    block_count = key_piece.shape[2] // tokens
    key_blocks = jnp.moveaxis(key_piece.reshape(samples, k_heads, block_count, tokens, HD), 2, 0)
    value_blocks = jnp.moveaxis(
        value_piece.reshape(samples, k_heads, block_count, tokens, HD), 2, 0
    )

    def step_block(carry, blocks):
        return (absorb(carry, blocks[0], blocks[1], 0.0), None)

    state_out, unused = lax.scan(step_block, state_now, (key_blocks, value_blocks))
    state_now = state_out
    best_old, weight_sum, accumulated = state_now
    attended = (accumulated / weight_sum[..., None]).astype(jnp.bfloat16)
    head_rows = attended.transpose(0, 3, 1, 2, 4).reshape(samples, tokens, q_width)
    projected_out = jnp.einsum(
        "srq,qd->srd",
        lax.all_to_all(head_rows, "tp", split_axis=1, concat_axis=2, tiled=True),
        w_out,
        preferred_element_type=jnp.float32,
    )
    return (latent.astype(jnp.float32) + gate_rows[:samples, None, :] * projected_out).astype(
        jnp.bfloat16
    )


def solution(mesh):
    placed = (
        P("dp", ("sp", "tp"), None),
        P("dp", "sp"),
        P("sp"),
        P("dp", "sp", None),
        P(),
        P("sp", "tp"),
        P("sp", "tp"),
        P("sp", "tp"),
        P(None, "tp"),
        P(None, "tp"),
        P(None, "tp"),
        P(),
        P(),
        P("tp"),
        P(),
    )
    return jax.shard_map(
        on_device,
        mesh=mesh,
        in_specs=placed,
        out_specs=P("dp", ("sp", "tp"), None),
        check_vma=False,
    )
```

profile of v0, /device:TPU:0, one launch (start us, length us, event | category | flops | bytes accessed | tf_op | source)
XLA Modules:
  0.0 190.3 jit_solution(14167755606228791362)
XLA Ops:
  10.9 20.5 %all-reduce = (f32[2,512]{1,0:T(2,128)S(1)}, f32[2,512]{1,0:T(2,128)S(1)}, f32[2,512]{1,0:T(2,128)S(1)}) all-reduce(f32[2,512]{1,0:T(2,128)S(1)} %fusion.94, f32[2,512]{1,0:T(2,128)S(1)} %fusion.96, f32[2,512]{1,0:T(2,128)S(1)} %fusion.98), channel_id=1, replica_groups=mesh['sp'=4,'tp'=4,'dp'=2] {'sp'}, use_global_device_ids=true, to_apply=%region_3.4 | all-reduce | flops 3072 | bytes 24576 | tf_op jit(solution)/shard_map/psum | solution.py:85
  31.4 8.2 %all_gather.25 = f32[2,2048]{1,0:T(2,128)S(1)} all-gather(f32[2,512]{1,0:T(2,128)S(1)} %get-tuple-element.88), channel_id=1, replica_groups=mesh['sp'=4,'tp'=4,'dp'=2] {'tp'}, dimensions={1}, use_global_device_ids=true | all-gather | bytes 20480 | tf_op jit(solution)/shard_map/all_gather | solution.py:86
  39.6 8.2 %all_gather.26 = f32[2,2048]{1,0:T(2,128)S(1)} all-gather(f32[2,512]{1,0:T(2,128)S(1)} %get-tuple-element.87), channel_id=1, replica_groups=mesh['sp'=4,'tp'=4,'dp'=2] {'tp'}, dimensions={1}, use_global_device_ids=true | all-gather | bytes 20480 | tf_op jit(solution)/shard_map/all_gather | solution.py:86
  49.8 2.4 %fusion.35 = bf16[1,192,2048]{2,1,0:T(8,128)(2,1)} fusion(bf16[1,192,2048]{2,1,0:T(8,128)(2,1)} %param.17, f32[2048]{0:T(1024)S(1)} %bitcast.173, f32[2048]{0:T(1024)S(1)} %bitcast.172, f32[2048]{0:T(1024)S(1)} %convert_element_type.119, f32[192]{0:T(256)S(1)} %add_rsqrt_fusion.2), kind=kLoop, calls=%fused_computation.39 | loop fusion | flops 2359296 | bytes 1598208 | tf_op jit(solution)/shard_map/convert_element_type | solution.py:19
  53.6 12.0 %all_gather.28 = bf16[1,1,512,64]{2,3,1,0:T(8,128)(2,1)S(1)} all-gather(bf16[1,1,128,64]{2,3,1,0:T(8,128)(2,1)S(1)} %fusion.77), channel_id=1, replica_groups=mesh['sp'=4,'tp'=4,'dp'=2] {'sp'}, dimensions={2}, use_global_device_ids=true | all-gather | bytes 81920 | tf_op jit(solution)/shard_map/all_gather | solution.py:144
  65.7 12.6 %all-gather = bf16[1,512,64]{1,2,0:T(8,128)(2,1)} all-gather(bf16[1,128,64]{1,2,0:T(8,128)(2,1)S(1)} %slice.80), channel_id=2, replica_groups=mesh['sp'=4,'tp'=4,'dp'=2] {'sp'}, dimensions={1}, use_global_device_ids=true | all-gather | bytes 81920 | tf_op jit(solution)/shard_map/all_gather | solution.py:145
  80.1 13.4 %all-gather.4.cloned.1.call-done = bf16[1,768,2048]{2,1,0:T(8,128)(2,1)} async-done(((bf16[1,192,2048]{2,1,0:T(8,128)(2,1)}), bf16[1,768,2048]{2,1,0:T(8,128)(2,1)}) %all-gather.4.cloned.1.call-update) | async-done | bytes 3145744 | tf_op jit(solution)/shard_map/all_gather | solution.py:96
  93.5 3.7 %fusion.41 = f32[1,768,384]{1,2,0:T(8,128)S(1)} fusion(bf16[2048,64]{1,0:T(8,128)(2,1)S(1)} %copy.47, bf16[2048,64]{1,0:T(8,128)(2,1)S(1)} %copy.46, bf16[2048,256]{1,0:T(8,128)(2,1)} %param.25, bf16[1,768,2048]{2,1,0:T(8,128)(2,1)} %all-gather.4.cloned.1.call-done), kind=kOutput, calls=%fused_computation.45 | convolution fusion | flops 1212678144 | bytes 5898240 | tf_op jit(solution)/shard_map/srd,dc->src/dot_general | solution.py:94
  101.3 14.6 %all_gather.30 = bf16[1,1,3072,64]{2,3,1,0:T(8,128)(2,1)S(1)} all-gather(bf16[1,1,768,64]{2,3,1,0:T(8,128)(2,1)S(1)} %convert_element_type.131), channel_id=1, replica_groups=mesh['sp'=4,'tp'=4,'dp'=2] {'sp'}, dimensions={2}, use_global_device_ids=true | all-gather | bytes 491520 | tf_op jit(solution)/shard_map/all_gather | solution.py:148
  117.0 2.6 %copy-done.1 = f32[4,768,512]{1,2,0:T(8,128)} copy-done((f32[4,768,512]{1,2,0:T(8,128)}, f32[4,768,512]{1,2,0:T(8,128)S(1)}, u32[]{:S(2)}) %copy-start.1) | copy-done | bytes 6291480
  120.9 15.5 %all-gather.1 = bf16[1,3072,64]{1,2,0:T(8,128)(2,1)S(1)} all-gather(bf16[1,768,64]{1,2,0:T(8,128)(2,1)S(1)} %slice.79), channel_id=3, replica_groups=mesh['sp'=4,'tp'=4,'dp'=2] {'sp'}, dimensions={1}, use_global_device_ids=true | all-gather | bytes 491520 | tf_op jit(solution)/shard_map/all_gather | solution.py:149
  136.8 4.3 %fusion.49 = f32[1,1,4,768,64]{3,4,2,1,0:T(8,128)S(1)} fusion(f32[4,768,512]{1,2,0:T(8,128)} %copy-done.1, f32[4,768]{1,0:T(4,128)S(1)} %get-tuple-element.106, f32[4]{0:T(128)S(1)} %copy-done.7, f32[4,768]{1,0:T(4,128)S(1)} %get-tuple-element.104, bf16[1,512,64]{1,2,0:T(8,128)(2,1)S(1)} %copy-done.6), kind=kOutput, calls=%fused_computation.49 | convolution fusion | flops 207814656 | bytes 7168016 | tf_op jit(solution)/shard_map/skgtr,skrd->skgtd/dot_general | solution.py:129
  141.0 19.7 %while.14 = (s32[]{:T(128)}, f32[1,1,4,768]{3,2,1,0:T(4,128)S(1)}, f32[1,1,4,768]{3,2,1,0:T(4,128)S(1)}, f32[1,1,4,768,64]{3,4,2,1,0:T(8,128)S(1)}, bf16[4,1,1,7...) while((s32[]{:T(128)}, f32[1,1,4,768]{3,2,1,0:T(4,128)S(1)}, ...), condition=%wide.region_13.14_spmd, body=%wide.region_10.13_spmd.sunk | while | flops 623256576 | bytes 30670940 | solution.py:159
  142.5 1.9 fusion.116
  144.4 1.6 fusion.115
  147.4 1.9 fusion.116
  149.3 1.6 fusion.115
  152.4 1.9 fusion.116
  157.3 1.9 fusion.116
  159.2 1.6 fusion.115
  162.0 3.0 %reduce.15 = bf16[768,256]{1,0:T(8,128)(2,1)S(1)} reduce(bf16[768,1,256]{2,1,0:T(2,128)(2,1)S(1)} %bitcast.162, bf16[]{:T(256)} %broadcast.433), dimensions={1}, to_apply=%bitcast.124.reduce_sub_computation | reduce | bytes 786434
  165.9 3.5 %all-to-all-start = ((bf16[4,2,24576]{2,1,0:T(2,128)(2,1)}), bf16[4,2,24576]{2,1,0:T(2,128)(2,1)S(1)}, u32[]{:S(2)}, u32[]{:S(2)}) async-start(bf16[4,2,24576]{2,1,0:T(2,128)(2,1)} %reshape.683), calls=%async_computation | async-start | bytes 786432 | tf_op jit(solution)/shard_map/all_to_all | solution.py:166
  169.4 9.1 %all_gather.24 = f32[2,2048]{1,0:T(2,128)S(1)} all-gather(f32[2,512]{1,0:T(2,128)S(1)} %get-tuple-element.89), channel_id=1, replica_groups=mesh['sp'=4,'tp'=4,'dp'=2] {'tp'}, dimensions={1}, use_global_device_ids=true | all-gather | bytes 20480 | tf_op jit(solution)/shard_map/all_gather | solution.py:86
  179.3 4.1 %fusion.30 = bf16[1,192,2048]{2,1,0:T(8,128)(2,1)} fusion(bf16[192,1024]{1,0:T(8,128)(2,1)S(1)} %bitcast.171, bf16[1024,2048]{1,0:T(8,128)(2,1)} %param.31, bf16[1,192,2048]{2,1,0:T(8,128)(2,1)S(1)} %copy-done.2, f32[2048]{0:T(1024)S(1)} %bitcast.174), kind=kOutput, calls=%fused_computation.32 | convolution fusion | flops 806879232 | bytes 6168576 | tf_op jit(solution)/shard_map/srq,qd->srd/dot_general | solution.py:164
  (100 shorter events, 26.6 us)
Async XLA Ops:
  6.5 1.0 copy-start
  6.5 45.7 %copy-start.5 = (bf16[2048,64]{0,1:T(8,128)(2,1)S(1)}, bf16[2048,64]{0,1:T(8,128)(2,1)}, u32[]{:S(2)}) copy-start(bf16[2048,64]{0,1:T(8,128)(2,1)} %param.26) | copy-start | bytes 786436
  6.5 46.0 %copy-start.4 = (bf16[2048,64]{0,1:T(8,128)(2,1)S(1)}, bf16[2048,64]{0,1:T(8,128)(2,1)}, u32[]{:S(2)}) copy-start(bf16[2048,64]{0,1:T(8,128)(2,1)} %param.27) | copy-start | bytes 786436
  6.5 46.3 %copy-start.8 = (bf16[64]{0:T(256)(128)(2,1)S(1)}, bf16[64]{0:T(256)(128)(2,1)}, u32[]{:S(2)}) copy-start(bf16[64]{0:T(256)(128)(2,1)} %param.29) | copy-start | bytes 388
  6.5 46.3 %copy-start.9 = (bf16[64]{0:T(256)(128)(2,1)S(1)}, bf16[64]{0:T(256)(128)(2,1)}, u32[]{:S(2)}) copy-start(bf16[64]{0:T(256)(128)(2,1)} %param.28) | copy-start | bytes 388
  6.5 46.3 %copy-start.3 = (bf16[1,128,2048]{2,1,0:T(8,128)(2,1)S(1)}, bf16[1,128,2048]{2,1,0:T(8,128)(2,1)}, u32[]{:S(2)}) copy-start(bf16[1,128,2048]{2,1,0:T(8,128)(2,1)} %param.20) | copy-start | bytes 1572868
  6.6 86.9 %all-gather.4.cloned.1.call-start = ((), (), s32[]{:S(2)}) async-start(), calls=%async_computation.1 | async-start | bytes 3932160 | tf_op jit(solution)/shard_map/all_gather | solution.py:96
  97.5 18.4 %copy-start.7 = (f32[4]{0:T(128)S(1)}, f32[4]{0:T(128)}, u32[]{:S(2)}) copy-start(f32[4]{0:T(128)} %param.30) | copy-start | bytes 52
  116.9 2.7 %copy-start.1 = (f32[4,768,512]{1,2,0:T(8,128)}, f32[4,768,512]{1,2,0:T(8,128)S(1)}, u32[]{:S(2)}) copy-start(f32[4,768,512]{1,2,0:T(8,128)S(1)} %get-tuple-element.114) | copy-start | bytes 18874372
  117.0 19.8 %copy-start.6 = (bf16[1,512,64]{1,2,0:T(8,128)(2,1)S(1)}, bf16[1,512,64]{1,2,0:T(8,128)(2,1)}, u32[]{:S(2)}) copy-start(bf16[1,512,64]{1,2,0:T(8,128)(2,1)} %all-gather) | copy-start | bytes 196612
  160.8 18.5 %copy-start.2 = (bf16[1,192,2048]{2,1,0:T(8,128)(2,1)S(1)}, bf16[1,192,2048]{2,1,0:T(8,128)(2,1)}, u32[]{:S(2)}) copy-start(bf16[1,192,2048]{2,1,0:T(8,128)(2,1)} %param.17) | copy-start | bytes 2359300
  165.9 12.5 %all-to-all-start = ((bf16[4,2,24576]{2,1,0:T(2,128)(2,1)}), bf16[4,2,24576]{2,1,0:T(2,128)(2,1)S(1)}, u32[]{:S(2)}, u32[]{:S(2)}) async-start(bf16[4,2,24576]{2,1,0:T(2,128)(2,1)} %reshape.683), calls=%async_computation | async-start | bytes 786432 | tf_op jit(solution)/shard_map/all_to_all | solution.py:166
Sparse Core Ops, SparseCore 0:
  52.3 41.0 all-gather.3
where the time goes:
time: 191 us; the launch traced here: 190 us
  blocking collectives  101 us (53%)
  matrix products  30 us (16%)
  other arithmetic  20 us (10%)
  between operations  13.8 us (7%)
  waiting for transfers between devices  13.4 us (7%)
  local copies, waits for them, and re-layouts  8.75 us (5%)
  starting transfers between devices  3.5 us (2%)
    all_gather x3, blocking collectives, on_device(): lax.all_gather(summed, 'tp', axis=1, tiled=True)  25.4 us
    psum x1, blocking collectives, on_device(): summed = lax.psum(partial_mods, 'sp')  20.5 us
    all_gather x1, blocking collectives, on_device(): value_piece = lax.all_gather(value_rows, 'sp', axis=2, tiled=True)  15.5 us
    all_gather x1, blocking collectives, on_device(): key_piece = lax.all_gather(key_rows, 'sp', axis=2, tiled=True)  14.6 us
    all_gather x1, waiting for transfers between devices, on_device(): lax.all_gather(modulated, 'tp', axis=1, tiled=True)  13.4 us
    all_gather x1, blocking collectives, on_device(): lax.all_gather(ctx_values, 'sp', axis=2, tiled=True)  12.6 us
    all_gather x1, blocking collectives, on_device(): lax.all_gather(ctx_keys, 'sp', axis=2, tiled=True)  12 us
    dot_general x5, matrix products, absorb(): jnp.einsum('skgtr,skrd->skgtd', weights.astype(jnp.bfloat16), value_block...  11.7 us
  transfers between devices with their start and end apart: 2, of which 1 were waited for; matrix products, arithmetic and copies ran while one was open for 2% of the time, Pallas kernels for 0%

commit v1 on v0

--- a/solution.py
+++ b/solution.py
@@ -7,6 +7,12 @@
 GRID_W = 128
 EPS = 1e-06
 THETA = 10000.0
+
+
+def in_order(pieces, dim):
+    shape = list(pieces.shape[1:])
+    shape[dim] *= pieces.shape[0]
+    return jnp.moveaxis(pieces, 0, dim).reshape(shape)
 
 
 def modulate(row_block, gain_vec, shift_rows, scale_rows):
@@ -91,12 +97,18 @@
     q_width = w_query.shape[1]
     k_width = w_key.shape[1]
     w_joint = jnp.concatenate([w_query, w_key, w_value], axis=1)
-    projected = jnp.einsum(
-        "srd,dc->src",
-        lax.all_gather(modulated, "tp", axis=1, tiled=True),
-        w_joint,
-        preferred_element_type=jnp.float32,
-    )
+    size, place, width_2 = (lax.axis_size("tp"), lax.axis_index("tp"), modulated.shape[1])
+    upward = [(i, (i + 1) % size) for i in range(size)]
+    parts = []
+    current = modulated
+    for step in range(size):
+        arriving = current if step == size - 1 else lax.ppermute(current, "tp", upward)
+        parts.append(
+            jnp.einsum("srd,dc->src", current, w_joint, preferred_element_type=jnp.float32)
+        )
+        current = arriving
+    parts = jnp.stack(parts)[(place - jnp.arange(size)) % size]
+    projected = in_order(parts, 1)
     tokens = projected.shape[1]
     k_heads = k_width // HD
     group_size = q_width // k_width

time: 191 us -> 192 us (level)
  between operations: 13.8 us -> 0.56 us
  waiting for transfers between devices: 13.4 us -> 25.1 us
  starting transfers between devices: 3.5 us -> 5.49 us
    ppermute x0 -> x3, waiting for transfers between devices: none -> 25.1 us  [on_device(): lax.ppermute(current, 'tp', upward)]
    all_gather x1 -> x0, waiting for transfers between devices: 13.4 us -> none  [on_device(): lax.all_gather(modulated, 'tp', axis=1, tiled=True)]
    ppermute x0 -> x3, starting transfers between devices: none -> 2.03 us  [on_device(): lax.ppermute(current, 'tp', upward)]
    dot_general x1 -> x4, matrix products: 3.66 us -> 5.26 us  [on_device(): jnp.einsum('srd,dc->src', current, w_joint, preferred_element_type=jnp.fl...]
    unnamed x27 -> x36, local copies, waits for them, and re-layouts: 5.28 us -> 4.57 us
  transfers between devices with their start and end apart: 2 -> 4, of which waited for: 1 -> 2; matrix products, arithmetic and copies ran while one was open for 2% -> 4% of each run, Pallas kernels for 0% -> 0%
where the time goes in v1:
time: 192 us; the launch traced here: 191 us
  blocking collectives  101 us (53%)
  matrix products  31.6 us (16%)
  waiting for transfers between devices  25.1 us (13%)
  other arithmetic  18.4 us (10%)
  local copies, waits for them, and re-layouts  9.01 us (5%)
  starting transfers between devices  5.49 us (3%)
    all_gather x3, blocking collectives, on_device(): lax.all_gather(summed, 'tp', axis=1, tiled=True)  25.5 us
    ppermute x3, waiting for transfers between devices, on_device(): lax.ppermute(current, 'tp', upward)  25.1 us
    psum x1, blocking collectives, on_device(): summed = lax.psum(partial_mods, 'sp')  20.5 us
    all_gather x1, blocking collectives, on_device(): key_piece = lax.all_gather(key_rows, 'sp', axis=2, tiled=True)  15.3 us
    all_gather x1, blocking collectives, on_device(): value_piece = lax.all_gather(value_rows, 'sp', axis=2, tiled=True)  14.6 us
    all_gather x1, blocking collectives, on_device(): lax.all_gather(ctx_values, 'sp', axis=2, tiled=True)  12.6 us
    all_gather x1, blocking collectives, on_device(): lax.all_gather(ctx_keys, 'sp', axis=2, tiled=True)  12.1 us
    dot_general x5, matrix products, absorb(): jnp.einsum('skgtr,skrd->skgtd', weights.astype(jnp.bfloat16), value_block...  11.7 us
  transfers between devices with their start and end apart: 4, of which 2 were waited for; matrix products, arithmetic and copies ran while one was open for 4% of the time, Pallas kernels for 0%

profile of v1, /device:TPU:0, one launch (start us, length us, event | category | flops | bytes accessed | tf_op | source)
XLA Modules:
  0.0 191.1 jit_solution(13506472082440747713)
XLA Ops:
  4.4 20.5 %all-reduce = (f32[2,512]{1,0:T(2,128)S(1)}, f32[2,512]{1,0:T(2,128)S(1)}, f32[2,512]{1,0:T(2,128)S(1)}) all-reduce(f32[2,512]{1,0:T(2,128)S(1)} %fusion.87, f32[2,512]{1,0:T(2,128)S(1)} %fusion.89, f32[2,512]{1,0:T(2,128)S(1)} %fusion.91), channel_id=1, replica_groups=mesh['sp'=4,'tp'=4,'dp'=2] {'sp'}, use_global_device_ids=true, to_apply=%region_3.4 | all-reduce | flops 3072 | bytes 24576 | tf_op jit(solution)/shard_map/psum | solution.py:91
  24.8 8.2 %all_gather.22 = f32[2,2048]{1,0:T(2,128)S(1)} all-gather(f32[2,512]{1,0:T(2,128)S(1)} %get-tuple-element.81), channel_id=1, replica_groups=mesh['sp'=4,'tp'=4,'dp'=2] {'tp'}, dimensions={1}, use_global_device_ids=true | all-gather | bytes 20480 | tf_op jit(solution)/shard_map/all_gather | solution.py:92
  33.0 8.2 %all_gather.23 = f32[2,2048]{1,0:T(2,128)S(1)} all-gather(f32[2,512]{1,0:T(2,128)S(1)} %get-tuple-element.80), channel_id=1, replica_groups=mesh['sp'=4,'tp'=4,'dp'=2] {'tp'}, dimensions={1}, use_global_device_ids=true | all-gather | bytes 20480 | tf_op jit(solution)/shard_map/all_gather | solution.py:92
  46.9 12.1 %all_gather.24 = bf16[1,1,512,64]{2,3,1,0:T(8,128)(2,1)S(1)} all-gather(bf16[1,1,128,64]{2,3,1,0:T(8,128)(2,1)S(1)} %fusion.69), channel_id=1, replica_groups=mesh['sp'=4,'tp'=4,'dp'=2] {'sp'}, dimensions={2}, use_global_device_ids=true | all-gather | bytes 81920 | tf_op jit(solution)/shard_map/all_gather | solution.py:156
  59.0 12.6 %all-gather = bf16[1,512,64]{1,2,0:T(8,128)(2,1)} all-gather(bf16[1,128,64]{1,2,0:T(8,128)(2,1)S(1)} %slice.77), channel_id=2, replica_groups=mesh['sp'=4,'tp'=4,'dp'=2] {'sp'}, dimensions={1}, use_global_device_ids=true | all-gather | bytes 81920 | tf_op jit(solution)/shard_map/all_gather | solution.py:157
  74.9 16.9 %collective-permute-done.1 = bf16[1,192,2048]{2,1,0:T(8,128)(2,1)S(1)} collective-permute-done((bf16[1,192,2048]{2,1,0:T(8,128)(2,1)}, bf16[1,192,2048]{2,1,0:T(8,128)(2,1)S(1)}, u32[]{:S(2)}, u32[]{:S(2)}) %collective-permute-start.1) | collective-permute-done | bytes 786464 | tf_op jit(solution)/shard_map/ppermute | solution.py:105
  91.8 1.8 convolution_bitcast_fusion.3
  93.7 2.2 %convolution_bitcast_fusion.2 = f32[1,1,192,384]{3,2,1,0:T(8,128)S(1)} fusion(bf16[1,192,2048]{2,1,0:T(8,128)(2,1)} %collective-permute-done, bf16[2048,64]{1,0:T(8,128)(2,1)S(1)} %copy.54, bf16[2048,64]{1,0:T(8,128)(2,1)S(1)} %copy.53, bf16[2048,256]{1,0:T(8,128)(2,1)} %param.25), kind=kOutput, calls=%fused_computation.47 | convolution fusion | flops 306708480 | bytes 2654208 | tf_op jit(solution)/shard_map/srd,dc->src/dot_general | solution.py:107
  96.5 8.2 %collective-permute-done.2 = bf16[1,192,2048]{2,1,0:T(8,128)(2,1)S(1)} collective-permute-done((bf16[1,192,2048]{2,1,0:T(8,128)(2,1)S(1)}, bf16[1,192,2048]{2,1,0:T(8,128)(2,1)S(1)}, u32[]{:S(2)}, u32[]{:S(2)}) %collective-permute-start.2) | collective-permute-done | bytes 786464 | tf_op jit(solution)/shard_map/ppermute | solution.py:105
  110.0 15.3 %all_gather.26 = bf16[1,1,3072,64]{2,3,1,0:T(8,128)(2,1)S(1)} all-gather(bf16[1,1,768,64]{2,3,1,0:T(8,128)(2,1)S(1)} %convert_element_type.131), channel_id=1, replica_groups=mesh['sp'=4,'tp'=4,'dp'=2] {'sp'}, dimensions={2}, use_global_device_ids=true | all-gather | bytes 491520 | tf_op jit(solution)/shard_map/all_gather | solution.py:160
  129.4 14.6 %all-gather.1 = bf16[1,3072,64]{1,2,0:T(8,128)(2,1)S(1)} all-gather(bf16[1,768,64]{1,2,0:T(8,128)(2,1)S(1)} %copy.72), channel_id=3, replica_groups=mesh['sp'=4,'tp'=4,'dp'=2] {'sp'}, dimensions={1}, use_global_device_ids=true | all-gather | bytes 491520 | tf_op jit(solution)/shard_map/all_gather | solution.py:161
  144.4 4.3 %fusion.37 = f32[1,1,4,768,64]{3,4,2,1,0:T(8,128)S(1)} fusion(f32[4,768,512]{1,2,0:T(8,128)} %copy-done.1, f32[4,768]{1,0:T(4,128)S(1)} %get-tuple-element.99, f32[4]{0:T(128)S(1)} %copy-done.9, f32[4,768]{1,0:T(4,128)S(1)} %get-tuple-element.97, bf16[1,512,64]{1,2,0:T(8,128)(2,1)S(1)} %copy-done.8), kind=kOutput, calls=%fused_computation.43 | convolution fusion | flops 207814656 | bytes 7168016 | tf_op jit(solution)/shard_map/skgtr,skrd->skgtd/dot_general | solution.py:141
  148.6 19.7 %while.14 = (s32[]{:T(128)}, f32[1,1,4,768]{3,2,1,0:T(4,128)S(1)}, f32[1,1,4,768]{3,2,1,0:T(4,128)S(1)}, f32[1,1,4,768,64]{3,4,2,1,0:T(8,128)S(1)}, bf16[4,1,1,7...) while((s32[]{:T(128)}, f32[1,1,4,768]{3,2,1,0:T(4,128)S(1)}, ...), condition=%wide.region_13.14_spmd, body=%wide.region_10.13_spmd.sunk | while | flops 623256576 | bytes 30670940 | solution.py:171
  150.1 1.9 fusion.109
  152.0 1.6 fusion.108
  155.0 1.9 fusion.109
  156.9 1.6 fusion.108
  160.0 1.9 fusion.109
  161.9 1.6 fusion.108
  164.9 1.9 fusion.109
  169.6 3.1 %reduce.15 = bf16[768,256]{1,0:T(8,128)(2,1)S(1)} reduce(bf16[768,1,256]{2,1,0:T(2,128)(2,1)S(1)} %bitcast.183, bf16[]{:T(256)} %broadcast.502), dimensions={1}, to_apply=%bitcast.141.reduce_sub_computation | reduce | bytes 786434
  173.5 3.5 %all-to-all-start = ((bf16[4,2,24576]{2,1,0:T(2,128)(2,1)}), bf16[4,2,24576]{2,1,0:T(2,128)(2,1)S(1)}, u32[]{:S(2)}, u32[]{:S(2)}) async-start(bf16[4,2,24576]{2,1,0:T(2,128)(2,1)} %reshape.762), calls=%async_computation | async-start | bytes 786432 | tf_op jit(solution)/shard_map/all_to_all | solution.py:178
  177.0 9.1 %all_gather.21 = f32[2,2048]{1,0:T(2,128)S(1)} all-gather(f32[2,512]{1,0:T(2,128)S(1)} %get-tuple-element.82), channel_id=1, replica_groups=mesh['sp'=4,'tp'=4,'dp'=2] {'tp'}, dimensions={1}, use_global_device_ids=true | all-gather | bytes 20480 | tf_op jit(solution)/shard_map/all_gather | solution.py:92
  187.0 4.1 %fusion.28 = bf16[1,192,2048]{2,1,0:T(8,128)(2,1)} fusion(bf16[192,1024]{1,0:T(8,128)(2,1)S(1)} %bitcast.192, bf16[1024,2048]{1,0:T(8,128)(2,1)} %param.31, bf16[1,192,2048]{2,1,0:T(8,128)(2,1)S(1)} %copy-done.2, f32[2048]{0:T(1024)S(1)} %bitcast.195), kind=kOutput, calls=%fused_computation.31 | convolution fusion | flops 806879232 | bytes 6168576 | tf_op jit(solution)/shard_map/srq,qd->srd/dot_general | solution.py:176
  (121 shorter events, 33.5 us)
Async XLA Ops:
  0.0 1.1 copy-start
  0.0 45.5 %copy-start.5 = (bf16[2048,64]{0,1:T(8,128)(2,1)S(1)}, bf16[2048,64]{0,1:T(8,128)(2,1)}, u32[]{:S(2)}) copy-start(bf16[2048,64]{0,1:T(8,128)(2,1)} %param.26) | copy-start | bytes 786436
  0.0 45.8 %copy-start.4 = (bf16[2048,64]{0,1:T(8,128)(2,1)S(1)}, bf16[2048,64]{0,1:T(8,128)(2,1)}, u32[]{:S(2)}) copy-start(bf16[2048,64]{0,1:T(8,128)(2,1)} %param.27) | copy-start | bytes 786436
  0.0 46.1 %copy-start.11 = (bf16[64]{0:T(256)(128)(2,1)S(1)}, bf16[64]{0:T(256)(128)(2,1)}, u32[]{:S(2)}) copy-start(bf16[64]{0:T(256)(128)(2,1)} %param.29) | copy-start | bytes 388
  0.0 46.1 %copy-start.12 = (bf16[64]{0:T(256)(128)(2,1)S(1)}, bf16[64]{0:T(256)(128)(2,1)}, u32[]{:S(2)}) copy-start(bf16[64]{0:T(256)(128)(2,1)} %param.28) | copy-start | bytes 388
  0.0 46.1 %copy-start.3 = (bf16[1,128,2048]{2,1,0:T(8,128)(2,1)S(1)}, bf16[1,128,2048]{2,1,0:T(8,128)(2,1)}, u32[]{:S(2)}) copy-start(bf16[1,128,2048]{2,1,0:T(8,128)(2,1)} %param.20) | copy-start | bytes 1572868
  44.9 26.7 %collective-permute-start = (bf16[1,192,2048]{2,1,0:T(8,128)(2,1)S(1)}, bf16[1,192,2048]{2,1,0:T(8,128)(2,1)}, u32[]{:S(2)}, u32[]{:S(2)}) collective-permute-start(bf16[1,192,2048]{2,1,0:T(8,128)(2,1)S(1)} %fusion.33), channel_id=1, source_target_pairs={{0,2},{2,4},{4,6},{6,0},{1,3},{3,5},{5,7},{7,1},{8,10},{10,12},{12... | collective-permute-start | bytes 2359304 | tf_op jit(solution)/shard_map/ppermute | solution.py:105
  71.6 20.2 %collective-permute-start.1 = (bf16[1,192,2048]{2,1,0:T(8,128)(2,1)}, bf16[1,192,2048]{2,1,0:T(8,128)(2,1)S(1)}, u32[]{:S(2)}, u32[]{:S(2)}) collective-permute-start(bf16[1,192,2048]{2,1,0:T(8,128)(2,1)} %collective-permute-done), channel_id=1, source_target_pairs={{0,2},{2,4},{4,6},{6,0},{1,3},{3,5},{5,7},{7,1},{8,10},{10,12},{12... | collective-permute-start | bytes 2359304 | tf_op jit(solution)/shard_map/ppermute | solution.py:105
  91.8 12.9 %collective-permute-start.2 = (bf16[1,192,2048]{2,1,0:T(8,128)(2,1)S(1)}, bf16[1,192,2048]{2,1,0:T(8,128)(2,1)S(1)}, u32[]{:S(2)}, u32[]{:S(2)}) collective-permute-start(bf16[1,192,2048]{2,1,0:T(8,128)(2,1)S(1)} %collective-permute-done.1), channel_id=1, source_target_pairs={{0,2},{2,4},{4,6},{6,0},{1,3},{3,5},{5,7},{7,1},{8,10},{10,12},{12... | collective-permute-start | bytes 2359304 | tf_op jit(solution)/shard_map/ppermute | solution.py:105
  93.6 2.2 %copy-start.10 = (bf16[2048,256]{1,0:T(8,128)(2,1)S(1)}, bf16[2048,256]{1,0:T(8,128)(2,1)}, u32[]{:S(2)}) copy-start(bf16[2048,256]{1,0:T(8,128)(2,1)} %param.25) | copy-start | bytes 3145732
  107.4 2.0 %copy-start.6 = (f32[1,1,768,16]{2,3,1,0:T(8,128)S(1)}, f32[1,1,768,16]{2,3,1,0:T(8,128)}, u32[]{:S(2)}) copy-start(f32[1,1,768,16]{2,3,1,0:T(8,128)} %get-tuple-element.100) | copy-start | bytes 147460
  107.4 2.0 %copy-start.7 = (f32[1,1,768,16]{2,3,1,0:T(8,128)S(1)}, f32[1,1,768,16]{2,3,1,0:T(8,128)}, u32[]{:S(2)}) copy-start(f32[1,1,768,16]{2,3,1,0:T(8,128)} %get-tuple-element.105) | copy-start | bytes 147460
  108.5 17.0 %copy-start.9 = (f32[4]{0:T(128)S(1)}, f32[4]{0:T(128)}, u32[]{:S(2)}) copy-start(f32[4]{0:T(128)} %param.30) | copy-start | bytes 52
  126.6 2.7 %copy-start.1 = (f32[4,768,512]{1,2,0:T(8,128)}, f32[4,768,512]{1,2,0:T(8,128)S(1)}, u32[]{:S(2)}) copy-start(f32[4,768,512]{1,2,0:T(8,128)S(1)} %get-tuple-element.107) | copy-start | bytes 18874372
  129.2 15.1 %copy-start.8 = (bf16[1,512,64]{1,2,0:T(8,128)(2,1)S(1)}, bf16[1,512,64]{1,2,0:T(8,128)(2,1)}, u32[]{:S(2)}) copy-start(bf16[1,512,64]{1,2,0:T(8,128)(2,1)} %all-gather) | copy-start | bytes 196612
  169.6 17.4 %copy-start.2 = (bf16[1,192,2048]{2,1,0:T(8,128)(2,1)S(1)}, bf16[1,192,2048]{2,1,0:T(8,128)(2,1)}, u32[]{:S(2)}) copy-start(bf16[1,192,2048]{2,1,0:T(8,128)(2,1)} %param.17) | copy-start | bytes 2359300
  173.5 12.5 %all-to-all-start = ((bf16[4,2,24576]{2,1,0:T(2,128)(2,1)}), bf16[4,2,24576]{2,1,0:T(2,128)(2,1)S(1)}, u32[]{:S(2)}, u32[]{:S(2)}) async-start(bf16[4,2,24576]{2,1,0:T(2,128)(2,1)} %reshape.762), calls=%async_computation | async-start | bytes 786432 | tf_op jit(solution)/shard_map/all_to_all | solution.py:178
